TPU v7x, 128 devices: a whole 4x4x4 slice. The times are simulated.
128 devices in a mesh: sp: 16 (over z, x), tp: 8 (over y, core).
Axes of the slice: x: 4, y: 4, z: 4, core: 2. Of those that a mesh axis runs over, the one named last changes fastest.
Arguments:
- query_narrow: bfloat16 [4096, 1024], P('sp', 'tp'), may hold values from -6 to 6
- key_narrow: bfloat16 [4096, 1024], P('sp', 'tp'), may hold values from -6 to 6
- value_narrow: bfloat16 [4096, 1024], P('sp', 'tp'), may hold values from -12 to 12
- query_broad: bfloat16 [4096, 1024], P('sp', 'tp'), may hold values from -6 to 6
- key_broad: bfloat16 [4096, 1024], P('sp', 'tp'), may hold values from -6 to 6
- value_broad: bfloat16 [4096, 1024], P('sp', 'tp'), may hold values from -12 to 12
- offset_narrow: bfloat16 [16, 4096], P('tp', 'sp'), as said below
- offset_broad: bfloat16 [8, 4096], P('tp', 'sp'), as said below
- residual: bfloat16 [4096, 2048], P(('sp', 'tp')), may hold values from -6 to 6
- out_narrow: bfloat16 [1024, 2048], P('tp'), may hold values from -0.25 to 0.25
- out_broad: bfloat16 [1024, 2048], P('tp'), may hold values from -0.25 to 0.25
- norm_gain: float32 [2048], replicated, may hold values from 0.1 to 1.9
- up_proj: bfloat16 [2048, 8192], P('sp', 'tp'), may hold values from -0.125 to 0.125
- down_proj: bfloat16 [8192, 2048], P('tp', 'sp'), may hold values from -0.0625 to 0.0625
Outputs:
- output: bfloat16 [4096, 2048], P(('sp', 'tp'))
Inputs may be any that keep to these rules, and one draw needn't show every extreme that they name: `offset_narrow`: additive score offsets of each head for each key position. `offset_broad`: additive score offsets of each head for each key position.
All inputs are finite; a program needn't handle non-finite values.
Results may differ from a plain program's by a relative error of at most 0.018.
Values may be sent and summed in bfloat16 or wider, within the bound.
A program may use at most 64 MiB of HBM per device.

v0:
```python
import math
import jax
import jax.numpy as jnp
from jax import lax
from jax.sharding import PartitionSpec as P

NARROW_SIZE = 64
BROAD_SIZE = 128


def turned_gather(arrays, axis, dims):
    turned = [jnp.moveaxis(a, dim, 0) for a, dim in zip(arrays, dims)]
    widths = [t[0].size for t in turned]
    both = jnp.concatenate([t.reshape(-1, w) for t, w in zip(turned, widths)], axis=1)
    whole = lax.all_gather(both, axis, axis=0, tiled=True)
    tiles = jnp.split(whole, [sum(widths[:k]) for k in range(1, len(widths))], axis=1)
    return tuple(
        (
            jnp.moveaxis(b.reshape(-1, *t.shape[1:]), 0, dim)
            for b, t, dim in zip(tiles, turned, dims)
        )
    )


def cut_along(value, dim, count):
    dims = value.shape
    tiles = value.reshape(*dims[:dim], count, dims[dim] // count, *dims[dim + 1 :])
    return jnp.moveaxis(tiles, dim, 0)


def summed_on_arrival(value, axis, dim):
    count = lax.axis_size(axis)
    tiles = lax.all_to_all(cut_along(value, dim, count), axis, 0, 0, tiled=True)
    return jnp.sum(tiles.astype(jnp.float32), axis=0)


def from_everyone(value, axis):
    copies = jnp.broadcast_to(value, (lax.axis_size(axis), *value.shape))
    return lax.all_to_all(copies, axis, split_axis=0, concat_axis=0, tiled=True)


def in_order(tiles, dim):
    dims = list(tiles.shape[1:])
    dims[dim] *= tiles.shape[0]
    return jnp.moveaxis(tiles, 0, dim).reshape(dims)


def collect(value, axis, dim):
    tiles = from_everyone(value, axis)
    return in_order(tiles, dim)


def on_gathered_pieces(value, axis, dim, work, out_dim):
    width = value.shape[dim]
    pieces = jnp.split(value, 2, axis=dim) if width % 2 == 0 else [value]
    leading = jnp.arange(lax.axis_size(axis)) * width
    tiles = [lax.all_gather(share, axis) for share in pieces]
    made = [jax.vmap(work)(b, leading + k * (width // len(pieces))) for k, b in enumerate(tiles)]
    return in_order(jnp.concatenate(made, axis=out_dim + 1), out_dim)


def stick_block(state, query, keys_block, values_block, offsets, query_pos, key_pos, head_size):
    keep_sum, running = state
    row_count = query.shape[0]
    total_heads = query.shape[1] // head_size
    key_count = keys_block.shape[0]
    q_heads = query.reshape(row_count, total_heads, head_size)
    k_heads = keys_block.reshape(key_count, total_heads, head_size)
    v_heads = values_block.reshape(key_count, total_heads, head_size)
    scores = jnp.einsum(
        "qhe,khe->hqk", q_heads, k_heads, preferred_element_type=jnp.float32
    ) * head_size ** (-0.5)
    scores = scores + offsets.astype(jnp.float32)[:, None, :]
    causal = (key_pos[None, :] < query_pos[:, None])[None]
    log_keep = jnp.where(causal, jax.nn.log_sigmoid(-scores), 0.0)
    keep_after = lax.cumsum(log_keep, axis=2, reverse=True) - log_keep
    weight = jnp.where(
        causal, jnp.exp(jax.nn.log_sigmoid(scores) + keep_after + keep_sum[:, :, None]), 0.0
    )
    weight = weight.astype(jnp.bfloat16)
    running = running + jnp.einsum(
        "hqk,khe->qhe", weight, v_heads, preferred_element_type=jnp.float32
    )
    return (keep_sum + jnp.sum(log_keep, axis=2), running)


def attend_block(states, pieces, query_pos, key_pos, queries):
    key_n, value_n, key_b, value_b, off_n, off_b = pieces
    state_narrow = stick_block(
        states[0], queries[0], key_n, value_n, off_n, query_pos, key_pos, NARROW_SIZE
    )
    state_broad = stick_block(
        states[1], queries[1], key_b, value_b, off_b, query_pos, key_pos, BROAD_SIZE
    )
    return (state_narrow, state_broad)


def local(
    query_narrow,
    key_narrow,
    value_narrow,
    query_broad,
    key_broad,
    value_broad,
    offset_narrow,
    offset_broad,
    residual,
    out_narrow,
    out_broad,
    norm_gain,
    up_proj,
    down_proj,
):
    tok_dev = query_narrow.shape[0]
    my_shard = lax.axis_index("sp")
    query_pos = my_shard * tok_dev + jnp.arange(tok_dev, dtype=jnp.int32)
    queries = (query_narrow, query_broad)

    def empty_state(total_heads, head_size):
        return (
            jnp.zeros((total_heads, tok_dev), jnp.float32),
            jnp.zeros((tok_dev, total_heads, head_size), jnp.float32),
        )

    states = (
        empty_state(offset_narrow.shape[0], NARROW_SIZE),
        empty_state(offset_broad.shape[0], BROAD_SIZE),
    )
    own_keys = (key_narrow, value_narrow, key_broad, value_broad, offset_narrow, offset_broad)
    whole_keys = turned_gather(
        (own_keys[0], own_keys[1], own_keys[2], own_keys[3], own_keys[4], own_keys[5]),
        "sp",
        (0, 0, 0, 0, 1, 1),
    )
    key_span = math.gcd(tok_dev, 512)
    block_count = (my_shard + 1) * (tok_dev // key_span)

    def sweep(turn_index, current):
        first_row = (block_count - 1 - turn_index) * key_span
        row_pieces = tuple(
            (lax.dynamic_slice_in_dim(array, first_row, key_span, 0) for array in whole_keys[:4])
        )
        col_pieces = tuple(
            (lax.dynamic_slice_in_dim(array, first_row, key_span, 1) for array in whole_keys[4:])
        )
        key_pos = first_row + jnp.arange(key_span, dtype=jnp.int32)
        return attend_block(current, row_pieces + col_pieces, query_pos, key_pos, queries)

    states = lax.fori_loop(0, block_count, sweep, states)
    mixed_narrow = states[0][1].reshape(tok_dev, -1).astype(jnp.bfloat16)
    mixed_broad = states[1][1].reshape(tok_dev, -1).astype(jnp.bfloat16)
    attended = summed_on_arrival(
        (
            jnp.dot(mixed_narrow, out_narrow, preferred_element_type=jnp.float32)
            + jnp.dot(mixed_broad, out_broad, preferred_element_type=jnp.float32)
        ).astype(jnp.bfloat16),
        "tp",
        0,
    )
    updated = residual.astype(jnp.float32) + attended
    scale = lax.rsqrt(jnp.mean(updated * updated, axis=-1, keepdims=True) + 1e-06)
    normed = (updated * scale * norm_gain).astype(jnp.bfloat16)
    gathered = collect(normed, "tp", 0)
    pre_act = jnp.dot(
        gathered,
        lax.all_gather(up_proj, "sp", axis=0, tiled=True),
        preferred_element_type=jnp.float32,
    )
    hidden = jnp.square(jax.nn.relu(pre_act)).astype(jnp.bfloat16)

    def project(shard_piece, row_start):
        return jnp.dot(hidden, shard_piece, preferred_element_type=jnp.float32)

    partial_sums = on_gathered_pieces(down_proj, "sp", 1, project, 1)
    channel = summed_on_arrival(partial_sums.astype(jnp.bfloat16), "tp", 0)
    return (updated + channel).astype(jnp.bfloat16)


def solution(mesh):
    return jax.shard_map(
        local,
        mesh=mesh,
        in_specs=(
            P("sp", "tp"),
            P("sp", "tp"),
            P("sp", "tp"),
            P("sp", "tp"),
            P("sp", "tp"),
            P("sp", "tp"),
            P("tp", "sp"),
            P("tp", "sp"),
            P(("sp", "tp"), None),
            P("tp", None),
            P("tp", None),
            P(),
            P("sp", "tp"),
            P("tp", "sp"),
        ),
        out_specs=P(("sp", "tp"), None),
        check_vma=False,
    )
```

profile of v0, /device:TPU:102, one launch (start us, length us, event | category | flops | bytes accessed | tf_op | source)
XLA Modules:
  0.0 342.0 jit_solution(4118133415750312991)
XLA Ops:
  8.2 1.8 concatenate.7
  10.1 1.9 fusion.43
  13.5 52.2 %all-gather.7.cloned.1.call-done = bf16[4096,515]{1,0:T(8,128)(2,1)} async-done(((bf16[256,515]{1,0:T(8,128)(2,1)}), bf16[4096,515]{1,0:T(8,128)(2,1)}) %all-gather.7.cloned.1.call-update) | async-done | bytes 4218896 | tf_op jit(solution)/shard_map/all_gather | solution.py:15
  65.7 1.3 slice_bitcast_fusion.3
  67.3 2.0 slice_reduce_fusion
  69.3 3.9 %fusion.42 = (bf16[4096,128]{1,0:T(8,128)(2,1)S(1)}, bf16[4096,128]{1,0:T(8,128)(2,1)}, bf16[4096,128]{1,0:T(8,128)(2,1)}, bf16[4096,128]{1,0:T(8,128)(2,1)}) fusion(bf16[4096,515]{1,0:T(8,128)(2,1)} %all-gather.7.cloned.1.call-done), kind=kLoop, calls=%fused_computation.76 | loop fusion | bytes 8388608 | tf_op jit(solution)/shard_map/split | solution.py:16
  73.3 191.5 %while.19 = (s32[]{:T(128)}, f32[2,256]{1,0:T(2,128)S(1)}, f32[256,2,64]{0,2,1:T(8,128)S(1)}, f32[1,256]{1,0:T(1,128)S(1)}, f32[256,1,128]{0,2,1:T(8,128)S(1)}, ...) while((s32[]{:T(128)}, f32[2,256]{1,0:T(2,128)S(1)}, ...), condition=%wide.region_7.8_spmd.clone, body=%wide.region_0.7_spmd.clone.sunk | while | flops 98831880 | bytes 9842459 | solution.py:149
  75.1 4.6 %fusion.92 = f32[2,256,2,128]{1,2,3,0:T(2,128)S(1)} fusion(f32[2,256,2,128]{1,3,2,0:T(8,128)S(1)} %bitcast.125), kind=kOutput, calls=%fused_computation.24.clone.1 | output fusion | flops 16646144 | bytes 1048576 | tf_op jit(solution)/shard_map/reduce-window.8
  81.1 1.2 fusion.96
  82.3 2.3 fusion.97
  87.0 4.6 %fusion.92 = f32[2,256,2,128]{1,2,3,0:T(2,128)S(1)} fusion(f32[2,256,2,128]{1,3,2,0:T(8,128)S(1)} %bitcast.125), kind=kOutput, calls=%fused_computation.24.clone.1 | output fusion | flops 16646144 | bytes 1048576 | tf_op jit(solution)/shard_map/reduce-window.8
  93.1 1.2 fusion.96
  94.3 2.3 fusion.97
  99.0 4.6 %fusion.92 = f32[2,256,2,128]{1,2,3,0:T(2,128)S(1)} fusion(f32[2,256,2,128]{1,3,2,0:T(8,128)S(1)} %bitcast.125), kind=kOutput, calls=%fused_computation.24.clone.1 | output fusion | flops 16646144 | bytes 1048576 | tf_op jit(solution)/shard_map/reduce-window.8
  105.0 1.2 fusion.96
  106.2 2.3 fusion.97
  111.0 4.6 %fusion.92 = f32[2,256,2,128]{1,2,3,0:T(2,128)S(1)} fusion(f32[2,256,2,128]{1,3,2,0:T(8,128)S(1)} %bitcast.125), kind=kOutput, calls=%fused_computation.24.clone.1 | output fusion | flops 16646144 | bytes 1048576 | tf_op jit(solution)/shard_map/reduce-window.8
  117.0 1.2 fusion.96
  118.2 2.3 fusion.97
  123.0 4.6 %fusion.92 = f32[2,256,2,128]{1,2,3,0:T(2,128)S(1)} fusion(f32[2,256,2,128]{1,3,2,0:T(8,128)S(1)} %bitcast.125), kind=kOutput, calls=%fused_computation.24.clone.1 | output fusion | flops 16646144 | bytes 1048576 | tf_op jit(solution)/shard_map/reduce-window.8
  129.0 1.2 fusion.96
  130.2 2.3 fusion.97
  134.9 4.6 %fusion.92 = f32[2,256,2,128]{1,2,3,0:T(2,128)S(1)} fusion(f32[2,256,2,128]{1,3,2,0:T(8,128)S(1)} %bitcast.125), kind=kOutput, calls=%fused_computation.24.clone.1 | output fusion | flops 16646144 | bytes 1048576 | tf_op jit(solution)/shard_map/reduce-window.8
  141.0 1.2 fusion.96
  142.2 2.3 fusion.97
  146.9 4.6 %fusion.92 = f32[2,256,2,128]{1,2,3,0:T(2,128)S(1)} fusion(f32[2,256,2,128]{1,3,2,0:T(8,128)S(1)} %bitcast.125), kind=kOutput, calls=%fused_computation.24.clone.1 | output fusion | flops 16646144 | bytes 1048576 | tf_op jit(solution)/shard_map/reduce-window.8
  152.9 1.2 fusion.96
  154.1 2.3 fusion.97
  158.9 4.6 %fusion.92 = f32[2,256,2,128]{1,2,3,0:T(2,128)S(1)} fusion(f32[2,256,2,128]{1,3,2,0:T(8,128)S(1)} %bitcast.125), kind=kOutput, calls=%fused_computation.24.clone.1 | output fusion | flops 16646144 | bytes 1048576 | tf_op jit(solution)/shard_map/reduce-window.8
  164.9 1.2 fusion.96
  166.1 2.3 fusion.97
  170.9 4.6 %fusion.92 = f32[2,256,2,128]{1,2,3,0:T(2,128)S(1)} fusion(f32[2,256,2,128]{1,3,2,0:T(8,128)S(1)} %bitcast.125), kind=kOutput, calls=%fused_computation.24.clone.1 | output fusion | flops 16646144 | bytes 1048576 | tf_op jit(solution)/shard_map/reduce-window.8
  176.9 1.2 fusion.96
  178.1 2.3 fusion.97
  182.8 4.6 %fusion.92 = f32[2,256,2,128]{1,2,3,0:T(2,128)S(1)} fusion(f32[2,256,2,128]{1,3,2,0:T(8,128)S(1)} %bitcast.125), kind=kOutput, calls=%fused_computation.24.clone.1 | output fusion | flops 16646144 | bytes 1048576 | tf_op jit(solution)/shard_map/reduce-window.8
  188.8 1.2 fusion.96
  190.0 2.3 fusion.97
  194.8 4.6 %fusion.92 = f32[2,256,2,128]{1,2,3,0:T(2,128)S(1)} fusion(f32[2,256,2,128]{1,3,2,0:T(8,128)S(1)} %bitcast.125), kind=kOutput, calls=%fused_computation.24.clone.1 | output fusion | flops 16646144 | bytes 1048576 | tf_op jit(solution)/shard_map/reduce-window.8
  200.8 1.2 fusion.96
  202.0 2.3 fusion.97
  206.8 4.6 %fusion.92 = f32[2,256,2,128]{1,2,3,0:T(2,128)S(1)} fusion(f32[2,256,2,128]{1,3,2,0:T(8,128)S(1)} %bitcast.125), kind=kOutput, calls=%fused_computation.24.clone.1 | output fusion | flops 16646144 | bytes 1048576 | tf_op jit(solution)/shard_map/reduce-window.8
  212.8 1.2 fusion.96
  214.0 2.3 fusion.97
  218.7 4.6 %fusion.92 = f32[2,256,2,128]{1,2,3,0:T(2,128)S(1)} fusion(f32[2,256,2,128]{1,3,2,0:T(8,128)S(1)} %bitcast.125), kind=kOutput, calls=%fused_computation.24.clone.1 | output fusion | flops 16646144 | bytes 1048576 | tf_op jit(solution)/shard_map/reduce-window.8
  224.7 1.2 fusion.96
  225.9 2.3 fusion.97
  230.7 4.6 %fusion.92 = f32[2,256,2,128]{1,2,3,0:T(2,128)S(1)} fusion(f32[2,256,2,128]{1,3,2,0:T(8,128)S(1)} %bitcast.125), kind=kOutput, calls=%fused_computation.24.clone.1 | output fusion | flops 16646144 | bytes 1048576 | tf_op jit(solution)/shard_map/reduce-window.8
  236.7 1.2 fusion.96
  237.9 2.3 fusion.97
  242.7 4.6 %fusion.92 = f32[2,256,2,128]{1,2,3,0:T(2,128)S(1)} fusion(f32[2,256,2,128]{1,3,2,0:T(8,128)S(1)} %bitcast.125), kind=kOutput, calls=%fused_computation.24.clone.1 | output fusion | flops 16646144 | bytes 1048576 | tf_op jit(solution)/shard_map/reduce-window.8
  248.7 1.2 fusion.96
  249.9 2.3 fusion.97
  254.6 4.6 %fusion.92 = f32[2,256,2,128]{1,2,3,0:T(2,128)S(1)} fusion(f32[2,256,2,128]{1,3,2,0:T(8,128)S(1)} %bitcast.125), kind=kOutput, calls=%fused_computation.24.clone.1 | output fusion | flops 16646144 | bytes 1048576 | tf_op jit(solution)/shard_map/reduce-window.8
  260.6 1.2 fusion.96
  261.8 2.3 fusion.97
  266.4 20.2 %all_to_all.15 = bf16[8,32,2048]{2,1,0:T(8,128)(2,1)S(1)} all-to-all(bf16[8,32,2048]{2,1,0:T(8,128)(2,1)S(1)} %bitcast.134), channel_id=1, replica_groups=mesh['sp'=16,'tp'=8] {'tp'}, dimensions={0} | all-to-all | bytes 2097152 | tf_op jit(solution)/shard_map/all_to_all | solution.py:33
  287.0 1.1 broadcast_in_dim.51
  288.1 4.4 %all-to-all-start.1 = ((bf16[8,32,2048]{2,1,0:T(8,128)(2,1)}), bf16[8,32,2048]{2,1,0:T(8,128)(2,1)}, u32[]{:S(2)}, u32[]{:S(2)}) async-start(bf16[8,32,2048]{2,1,0:T(8,128)(2,1)} %broadcast_in_dim.51), calls=%async_computation.1 | async-start | bytes 2097152 | tf_op jit(solution)/shard_map/all_to_all | solution.py:39
  292.6 3.5 %copy.37 = bf16[16,1024,64]{1,2,0:T(8,128)(2,1)S(1)} copy(bf16[16,1024,64]{2,1,0:T(8,128)(2,1)} %bitcast.132) | data formatting | bytes 4194304 | tf_op jit(solution)/shard_map/all_gather | solution.py:57
  296.1 4.8 %copy.39 = bf16[16,1024,64]{1,2,0:T(8,128)(2,1)} copy(bf16[16,1024,64]{2,1,0:T(8,128)(2,1)} %bitcast.133) | data formatting | bytes 4194304 | tf_op jit(solution)/shard_map/all_gather | solution.py:57
  300.9 7.4 %all-to-all-done.1 = bf16[8,32,2048]{2,1,0:T(8,128)(2,1)} async-done(((bf16[8,32,2048]{2,1,0:T(8,128)(2,1)}), bf16[8,32,2048]{2,1,0:T(8,128)(2,1)}, u32[]{:S(2)}, u32[]{:S(2)}) %all-to-all-start.1) | async-done | bytes 1048608 | tf_op jit(solution)/shard_map/all_to_all | solution.py:39
  308.3 3.8 %fusion.39 = bf16[256,1024]{1,0:T(8,128)(2,1)S(1)} fusion(bf16[256,2048]{1,0:T(8,128)(2,1)} %bitcast.6, bf16[2048,1024]{1,0:T(8,128)(2,1)} %all-gather.9.cloned.1.call-done), kind=kOutput, calls=%fused_computation.63 | convolution fusion | flops 1074528256 | bytes 5767168 | tf_op jit(solution)/shard_map/dot_general | solution.py:164
  314.6 1.1 copy.40
  316.2 18.4 %all_to_all.16 = bf16[8,32,2048]{2,1,0:T(8,128)(2,1)S(1)} all-to-all(bf16[8,32,2048]{2,1,0:T(8,128)(2,1)S(1)} %convert_element_type.70), channel_id=1, replica_groups=mesh['sp'=16,'tp'=8] {'tp'}, dimensions={0} | all-to-all | bytes 2097152 | tf_op jit(solution)/shard_map/all_to_all | solution.py:33
  (416 shorter events, 69.2 us)
Async XLA Ops:
  6.5 258.4 %copy-start = (bf16[128,2048]{1,0:T(8,128)(2,1)S(1)}, bf16[128,2048]{1,0:T(8,128)(2,1)}, u32[]{:S(2)}) copy-start(bf16[128,2048]{1,0:T(8,128)(2,1)} %param.25) | copy-start | bytes 1572868
  6.5 6.8 %copy-start.4 = (bf16[256,128]{1,0:T(8,128)(2,1)S(1)}, bf16[256,128]{1,0:T(8,128)(2,1)}, u32[]{:S(2)}) copy-start(bf16[256,128]{1,0:T(8,128)(2,1)} %param.16) | copy-start | bytes 196612
  6.5 59.1 %all-gather.7.cloned.1.call-start = ((), (), s32[]{:S(2)}) async-start(), calls=%async_computation.3 | async-start | bytes 5570560 | tf_op jit(solution)/shard_map/all_gather | solution.py:15
  10.0 282.5 %all-gather.11.cloned.1.call-start = ((), (), s32[]{:S(2)}) async-start(), calls=%async_computation.5 | async-start | bytes 4456448 | tf_op jit(solution)/shard_map/all_gather | solution.py:57
  12.0 284.1 %all-gather.13.cloned.1.call-start = ((), (), s32[]{:S(2)}) async-start(), calls=%async_computation.6 | async-start | bytes 4456448 | tf_op jit(solution)/shard_map/all_gather | solution.py:57
  12.8 288.2 %all-gather.9.cloned.1.call-start = ((), (), s32[]{:S(2)}) async-start(), calls=%async_computation.4 | async-start | bytes 4456448 | tf_op jit(solution)/shard_map/all_gather | solution.py:166
  69.3 4.0 %copy-start.6 = (bf16[256,128]{1,0:T(8,128)(2,1)S(1)}, bf16[256,128]{1,0:T(8,128)(2,1)}, u32[]{:S(2)}) copy-start(bf16[256,128]{1,0:T(8,128)(2,1)} %param.19) | copy-start | bytes 196612
  264.9 1.0 copy-start.3
  266.4 20.4 %copy-start.2 = (bf16[32,2048]{1,0:T(8,128)(2,1)S(1)}, bf16[32,2048]{1,0:T(8,128)(2,1)}, u32[]{:S(2)}) copy-start(bf16[32,2048]{1,0:T(8,128)(2,1)} %param.24) | copy-start | bytes 393220
  266.4 20.5 %copy-start.5 = (f32[2048]{0:T(1024)S(1)}, f32[2048]{0:T(1024)}, u32[]{:S(2)}) copy-start(f32[2048]{0:T(1024)} %param.27) | copy-start | bytes 24580
  288.1 20.2 %all-to-all-start.1 = ((bf16[8,32,2048]{2,1,0:T(8,128)(2,1)}), bf16[8,32,2048]{2,1,0:T(8,128)(2,1)}, u32[]{:S(2)}, u32[]{:S(2)}) async-start(bf16[8,32,2048]{2,1,0:T(8,128)(2,1)} %broadcast_in_dim.51), calls=%async_computation.1 | async-start | bytes 2097152 | tf_op jit(solution)/shard_map/all_to_all | solution.py:39
  312.1 1.6 copy-start.1
Sparse Core Ops, SparseCore 0:
  10.2 55.4 all-gather.6
  67.8 51.0 all-gather.10
  121.1 51.0 all-gather.12
  174.2 51.0 all-gather.8
where the time goes:
time: 344 us; the launch traced here: 342 us
  other arithmetic  137 us (40%)
  waiting for transfers between devices  60.9 us (18%)
  local copies, waits for them, and re-layouts  44.4 us (13%)
  matrix products  40.3 us (12%)
  blocking collectives  38.6 us (11%)
  between operations  13.4 us (4%)
  starting transfers between devices  4.56 us (1%)
    another operation x64, other arithmetic  111 us
    all_gather x1, waiting for transfers between devices, turned_gather(): whole = lax.all_gather(both, axis, axis=0, tiled=True)  52.2 us
    all_to_all x2, blocking collectives, summed_on_arrival(): tiles = lax.all_to_all(cut_along(value, dim, count), axis, 0, 0, tiled=True)  38.6 us
    dot_general x32, matrix products, stick_block(): jnp.einsum('qhe,khe->hqk', q_heads, k_heads, preferred_element_type=jnp.f...  28 us
    convert_element_type x32, other arithmetic, stick_block(): weight = weight.astype(jnp.bfloat16)  19.2 us
    dynamic_slice x48, local copies, waits for them, and re-layouts, sweep(): lax.dynamic_slice_in_dim(array, first_row, key_span, 0)  17.7 us
    all_gather x2, local copies, waits for them, and re-layouts, on_gathered_pieces(): tiles = [lax.all_gather(share, axis) for share in pieces]  8.29 us
    all_to_all x1, waiting for transfers between devices, from_everyone(): return lax.all_to_all(copies, axis, split_axis=0, concat_axis=0, tiled=True)  7.39 us
  transfers between devices with their start and end apart: 5, of which 2 were waited for; matrix products, arithmetic and copies ran while one was open for 61% of the time, Pallas kernels for 0%

commit v1 on v0

--- a/solution.py
+++ b/solution.py
@@ -12,7 +12,9 @@
     turned = [jnp.moveaxis(a, dim, 0) for a, dim in zip(arrays, dims)]
     widths = [t[0].size for t in turned]
     both = jnp.concatenate([t.reshape(-1, w) for t, w in zip(turned, widths)], axis=1)
-    whole = lax.all_gather(both, axis, axis=0, tiled=True)
+    whole = jnp.concatenate(
+        lax.all_to_all(jnp.stack([both] * lax.axis_size(axis)), axis, 0, 0), axis=0
+    )
     tiles = jnp.split(whole, [sum(widths[:k]) for k in range(1, len(widths))], axis=1)
     return tuple(
         (

time: 344 us -> 363 us (1.055)
  waiting for transfers between devices: 60.9 us -> 72.5 us
  starting transfers between devices: 4.56 us -> 11.6 us
    all_to_all x0 -> x1, waiting for transfers between devices: none -> 63.7 us  [turned_gather(): lax.all_to_all(jnp.stack([both] * lax.axis_size(axis)), axis, 0, 0)]
    all_gather x1 -> x0, waiting for transfers between devices: 52.2 us -> none  [turned_gather(): whole = lax.all_gather(both, axis, axis=0, tiled=True)]
    all_to_all x0 -> x1, starting transfers between devices: none -> 7.04 us  [turned_gather(): lax.all_to_all(jnp.stack([both] * lax.axis_size(axis)), axis, 0, 0)]
    split x2 -> x1, local copies, waits for them, and re-layouts: 5.9 us -> 1.79 us  [turned_gather(): jnp.split(whole, [sum(widths[:k]) for k in range(1, len(widths))], axis=1)]
    dynamic_slice x48 -> x16, local copies, waits for them, and re-layouts: 17.7 us -> 14.2 us  [sweep(): lax.dynamic_slice_in_dim(array, first_row, key_span, 0)]
  transfers between devices with their start and end apart: 5 -> 5, of which waited for: 2 -> 2; matrix products, arithmetic and copies ran while one was open for 61% -> 58% of each run, Pallas kernels for 0% -> 0%
where the time goes in v1:
time: 363 us; the launch traced here: 360 us
  other arithmetic  137 us (38%)
  waiting for transfers between devices  72.5 us (20%)
  local copies, waits for them, and re-layouts  43.3 us (12%)
  matrix products  40.1 us (11%)
  blocking collectives  39.6 us (11%)
  between operations  13.4 us (4%)
  starting transfers between devices  11.6 us (3%)
    another operation x64, other arithmetic  111 us
    all_to_all x1, waiting for transfers between devices, turned_gather(): lax.all_to_all(jnp.stack([both] * lax.axis_size(axis)), axis, 0, 0)  63.7 us
    all_to_all x2, blocking collectives, summed_on_arrival(): tiles = lax.all_to_all(cut_along(value, dim, count), axis, 0, 0, tiled=True)  39.6 us
    dot_general x32, matrix products, stick_block(): jnp.einsum('qhe,khe->hqk', q_heads, k_heads, preferred_element_type=jnp.f...  28.3 us
    convert_element_type x32, other arithmetic, stick_block(): weight = weight.astype(jnp.bfloat16)  19.2 us
    dynamic_slice x16, local copies, waits for them, and re-layouts, sweep(): lax.dynamic_slice_in_dim(array, first_row, key_span, 0)  14.2 us
    all_gather x2, local copies, waits for them, and re-layouts, on_gathered_pieces(): tiles = [lax.all_gather(share, axis) for share in pieces]  8.32 us
    all_to_all x1, waiting for transfers between devices, from_everyone(): return lax.all_to_all(copies, axis, split_axis=0, concat_axis=0, tiled=True)  7.33 us
  transfers between devices with their start and end apart: 5, of which 2 were waited for; matrix products, arithmetic and copies ran while one was open for 58% of the time, Pallas kernels for 0%

profile of v1, /device:TPU:102, one launch (start us, length us, event | category | flops | bytes accessed | tf_op | source)
XLA Modules:
  0.0 360.4 jit_solution(2832424891438423362)
XLA Ops:
  6.5 2.0 fusion.43
  11.4 2.3 stack.2
  13.7 7.0 %all-to-all-start = ((bf16[16,256,515]{1,2,0:T(8,128)(2,1)}), bf16[16,256,515]{1,2,0:T(8,128)(2,1)}, u32[]{:S(2)}, u32[]{:S(2)}) async-start(bf16[16,256,515]{1,2,0:T(8,128)(2,1)} %stack.2), calls=%async_computation | async-start | bytes 8519680 | tf_op jit(solution)/shard_map/all_to_all | solution.py:16
  22.3 63.7 %all-to-all-done = bf16[16,256,515]{1,2,0:T(8,128)(2,1)} async-done(((bf16[16,256,515]{1,2,0:T(8,128)(2,1)}), bf16[16,256,515]{1,2,0:T(8,128)(2,1)}, u32[]{:S(2)}, u32[]{:S(2)}) %all-to-all-start) | async-done | bytes 4218912 | tf_op jit(solution)/shard_map/all_to_all | solution.py:16
  86.1 3.1 copy.88
  89.5 3.0 copy.82
  92.4 1.8 fusion.42
  94.4 187.8 %while.19 = (s32[]{:T(128)}, f32[2,256]{1,0:T(2,128)S(1)}, f32[256,2,64]{0,2,1:T(8,128)S(1)}, f32[1,256]{1,0:T(1,128)S(1)}, f32[256,1,128]{0,2,1:T(8,128)S(1)}, ...) while((s32[]{:T(128)}, f32[2,256]{1,0:T(2,128)S(1)}, ...), condition=%wide.region_7.8_spmd.clone, body=%wide.region_0.7_spmd.clone.sunk | while | flops 98831880 | bytes 9580315 | solution.py:151
  96.2 4.6 %fusion.92 = f32[2,256,2,128]{1,2,3,0:T(2,128)S(1)} fusion(f32[2,256,2,128]{1,3,2,0:T(8,128)S(1)} %bitcast.139), kind=kOutput, calls=%fused_computation.24.clone.1 | output fusion | flops 16646144 | bytes 1048576 | tf_op jit(solution)/shard_map/reduce-window.8
  102.1 1.2 fusion.96
  103.3 2.3 fusion.97
  107.9 4.6 %fusion.92 = f32[2,256,2,128]{1,2,3,0:T(2,128)S(1)} fusion(f32[2,256,2,128]{1,3,2,0:T(8,128)S(1)} %bitcast.139), kind=kOutput, calls=%fused_computation.24.clone.1 | output fusion | flops 16646144 | bytes 1048576 | tf_op jit(solution)/shard_map/reduce-window.8
  113.8 1.2 fusion.96
  115.0 2.3 fusion.97
  119.6 4.6 %fusion.92 = f32[2,256,2,128]{1,2,3,0:T(2,128)S(1)} fusion(f32[2,256,2,128]{1,3,2,0:T(8,128)S(1)} %bitcast.139), kind=kOutput, calls=%fused_computation.24.clone.1 | output fusion | flops 16646144 | bytes 1048576 | tf_op jit(solution)/shard_map/reduce-window.8
  125.5 1.2 fusion.96
  126.7 2.3 fusion.97
  131.3 4.6 %fusion.92 = f32[2,256,2,128]{1,2,3,0:T(2,128)S(1)} fusion(f32[2,256,2,128]{1,3,2,0:T(8,128)S(1)} %bitcast.139), kind=kOutput, calls=%fused_computation.24.clone.1 | output fusion | flops 16646144 | bytes 1048576 | tf_op jit(solution)/shard_map/reduce-window.8
  137.2 1.2 fusion.96
  138.5 2.3 fusion.97
  143.1 4.6 %fusion.92 = f32[2,256,2,128]{1,2,3,0:T(2,128)S(1)} fusion(f32[2,256,2,128]{1,3,2,0:T(8,128)S(1)} %bitcast.139), kind=kOutput, calls=%fused_computation.24.clone.1 | output fusion | flops 16646144 | bytes 1048576 | tf_op jit(solution)/shard_map/reduce-window.8
  149.0 1.2 fusion.96
  150.2 2.3 fusion.97
  154.8 4.6 %fusion.92 = f32[2,256,2,128]{1,2,3,0:T(2,128)S(1)} fusion(f32[2,256,2,128]{1,3,2,0:T(8,128)S(1)} %bitcast.139), kind=kOutput, calls=%fused_computation.24.clone.1 | output fusion | flops 16646144 | bytes 1048576 | tf_op jit(solution)/shard_map/reduce-window.8
  160.7 1.2 fusion.96
  161.9 2.3 fusion.97
  166.5 4.6 %fusion.92 = f32[2,256,2,128]{1,2,3,0:T(2,128)S(1)} fusion(f32[2,256,2,128]{1,3,2,0:T(8,128)S(1)} %bitcast.139), kind=kOutput, calls=%fused_computation.24.clone.1 | output fusion | flops 16646144 | bytes 1048576 | tf_op jit(solution)/shard_map/reduce-window.8
  172.4 1.2 fusion.96
  173.7 2.3 fusion.97
  178.3 4.6 %fusion.92 = f32[2,256,2,128]{1,2,3,0:T(2,128)S(1)} fusion(f32[2,256,2,128]{1,3,2,0:T(8,128)S(1)} %bitcast.139), kind=kOutput, calls=%fused_computation.24.clone.1 | output fusion | flops 16646144 | bytes 1048576 | tf_op jit(solution)/shard_map/reduce-window.8
  184.2 1.2 fusion.96
  185.4 2.3 fusion.97
  190.0 4.6 %fusion.92 = f32[2,256,2,128]{1,2,3,0:T(2,128)S(1)} fusion(f32[2,256,2,128]{1,3,2,0:T(8,128)S(1)} %bitcast.139), kind=kOutput, calls=%fused_computation.24.clone.1 | output fusion | flops 16646144 | bytes 1048576 | tf_op jit(solution)/shard_map/reduce-window.8
  195.9 1.2 fusion.96
  197.1 2.3 fusion.97
  201.7 4.6 %fusion.92 = f32[2,256,2,128]{1,2,3,0:T(2,128)S(1)} fusion(f32[2,256,2,128]{1,3,2,0:T(8,128)S(1)} %bitcast.139), kind=kOutput, calls=%fused_computation.24.clone.1 | output fusion | flops 16646144 | bytes 1048576 | tf_op jit(solution)/shard_map/reduce-window.8
  207.6 1.2 fusion.96
  208.8 2.3 fusion.97
  213.5 4.6 %fusion.92 = f32[2,256,2,128]{1,2,3,0:T(2,128)S(1)} fusion(f32[2,256,2,128]{1,3,2,0:T(8,128)S(1)} %bitcast.139), kind=kOutput, calls=%fused_computation.24.clone.1 | output fusion | flops 16646144 | bytes 1048576 | tf_op jit(solution)/shard_map/reduce-window.8
  219.4 1.2 fusion.96
  220.6 2.3 fusion.97
  225.2 4.6 %fusion.92 = f32[2,256,2,128]{1,2,3,0:T(2,128)S(1)} fusion(f32[2,256,2,128]{1,3,2,0:T(8,128)S(1)} %bitcast.139), kind=kOutput, calls=%fused_computation.24.clone.1 | output fusion | flops 16646144 | bytes 1048576 | tf_op jit(solution)/shard_map/reduce-window.8
  231.1 1.2 fusion.96
  232.3 2.3 fusion.97
  236.9 4.6 %fusion.92 = f32[2,256,2,128]{1,2,3,0:T(2,128)S(1)} fusion(f32[2,256,2,128]{1,3,2,0:T(8,128)S(1)} %bitcast.139), kind=kOutput, calls=%fused_computation.24.clone.1 | output fusion | flops 16646144 | bytes 1048576 | tf_op jit(solution)/shard_map/reduce-window.8
  242.8 1.2 fusion.96
  244.0 2.3 fusion.97
  248.6 4.6 %fusion.92 = f32[2,256,2,128]{1,2,3,0:T(2,128)S(1)} fusion(f32[2,256,2,128]{1,3,2,0:T(8,128)S(1)} %bitcast.139), kind=kOutput, calls=%fused_computation.24.clone.1 | output fusion | flops 16646144 | bytes 1048576 | tf_op jit(solution)/shard_map/reduce-window.8
  254.5 1.2 fusion.96
  255.8 2.3 fusion.97
  260.4 4.6 %fusion.92 = f32[2,256,2,128]{1,2,3,0:T(2,128)S(1)} fusion(f32[2,256,2,128]{1,3,2,0:T(8,128)S(1)} %bitcast.139), kind=kOutput, calls=%fused_computation.24.clone.1 | output fusion | flops 16646144 | bytes 1048576 | tf_op jit(solution)/shard_map/reduce-window.8
  266.3 1.2 fusion.96
  267.5 2.3 fusion.97
  272.1 4.6 %fusion.92 = f32[2,256,2,128]{1,2,3,0:T(2,128)S(1)} fusion(f32[2,256,2,128]{1,3,2,0:T(8,128)S(1)} %bitcast.139), kind=kOutput, calls=%fused_computation.24.clone.1 | output fusion | flops 16646144 | bytes 1048576 | tf_op jit(solution)/shard_map/reduce-window.8
  278.0 1.2 fusion.96
  279.2 2.3 fusion.97
  283.7 21.2 %all_to_all.20 = bf16[8,32,2048]{2,1,0:T(8,128)(2,1)S(1)} all-to-all(bf16[8,32,2048]{2,1,0:T(8,128)(2,1)S(1)} %bitcast.148), channel_id=1, replica_groups=mesh['sp'=16,'tp'=8] {'tp'}, dimensions={0} | all-to-all | bytes 2097152 | tf_op jit(solution)/shard_map/all_to_all | solution.py:35
  305.4 1.1 broadcast_in_dim.51
  306.5 4.5 %all-to-all-start.2 = ((bf16[8,32,2048]{2,1,0:T(8,128)(2,1)}), bf16[8,32,2048]{2,1,0:T(8,128)(2,1)}, u32[]{:S(2)}, u32[]{:S(2)}) async-start(bf16[8,32,2048]{2,1,0:T(8,128)(2,1)} %broadcast_in_dim.51), calls=%async_computation.2 | async-start | bytes 2097152 | tf_op jit(solution)/shard_map/all_to_all | solution.py:41
  311.0 3.5 copy.71
  314.6 4.8 %copy.73 = bf16[16,1024,64]{1,2,0:T(8,128)(2,1)} copy(bf16[16,1024,64]{2,1,0:T(8,128)(2,1)} %bitcast.147) | data formatting | bytes 4194304 | tf_op jit(solution)/shard_map/all_gather | solution.py:59
  319.3 7.3 %all-to-all-done.2 = bf16[8,32,2048]{2,1,0:T(8,128)(2,1)} async-done(((bf16[8,32,2048]{2,1,0:T(8,128)(2,1)}), bf16[8,32,2048]{2,1,0:T(8,128)(2,1)}, u32[]{:S(2)}, u32[]{:S(2)}) %all-to-all-start.2) | async-done | bytes 1048608 | tf_op jit(solution)/shard_map/all_to_all | solution.py:41
  326.7 3.8 %fusion.39 = bf16[256,1024]{1,0:T(8,128)(2,1)S(1)} fusion(bf16[256,2048]{1,0:T(8,128)(2,1)} %bitcast.7, bf16[2048,1024]{1,0:T(8,128)(2,1)} %all-gather.6.cloned.1.call-done), kind=kOutput, calls=%fused_computation.64 | convolution fusion | flops 1074528256 | bytes 5767168 | tf_op jit(solution)/shard_map/dot_general | solution.py:166
  334.6 18.4 %all_to_all.21 = bf16[8,32,2048]{2,1,0:T(8,128)(2,1)S(1)} all-to-all(bf16[8,32,2048]{2,1,0:T(8,128)(2,1)S(1)} %convert_element_type.70), channel_id=1, replica_groups=mesh['sp'=16,'tp'=8] {'tp'}, dimensions={0} | all-to-all | bytes 2097152 | tf_op jit(solution)/shard_map/all_to_all | solution.py:35
  (386 shorter events, 67.5 us)
Async XLA Ops:
  6.5 275.7 %copy-start = (bf16[128,2048]{1,0:T(8,128)(2,1)S(1)}, bf16[128,2048]{1,0:T(8,128)(2,1)}, u32[]{:S(2)}) copy-start(bf16[128,2048]{1,0:T(8,128)(2,1)} %param.25) | copy-start | bytes 1572868
  6.5 304.4 %all-gather.8.cloned.1.call-start = ((), (), s32[]{:S(2)}) async-start(), calls=%async_computation.5 | async-start | bytes 4456448 | tf_op jit(solution)/shard_map/all_gather | solution.py:59
  13.7 8.5 %copy-start.4 = (bf16[256,128]{1,0:T(8,128)(2,1)S(1)}, bf16[256,128]{1,0:T(8,128)(2,1)}, u32[]{:S(2)}) copy-start(bf16[256,128]{1,0:T(8,128)(2,1)} %param.16) | copy-start | bytes 196612
  13.7 72.4 %all-to-all-start = ((bf16[16,256,515]{1,2,0:T(8,128)(2,1)}), bf16[16,256,515]{1,2,0:T(8,128)(2,1)}, u32[]{:S(2)}, u32[]{:S(2)}) async-start(bf16[16,256,515]{1,2,0:T(8,128)(2,1)} %stack.2), calls=%async_computation | async-start | bytes 8519680 | tf_op jit(solution)/shard_map/all_to_all | solution.py:16
  20.7 293.9 %all-gather.10.cloned.1.call-start = ((), (), s32[]{:S(2)}) async-start(), calls=%async_computation.6 | async-start | bytes 4456448 | tf_op jit(solution)/shard_map/all_gather | solution.py:59
  21.4 305.2 %all-gather.6.cloned.1.call-start = ((), (), s32[]{:S(2)}) async-start(), calls=%async_computation.4 | async-start | bytes 4456448 | tf_op jit(solution)/shard_map/all_gather | solution.py:168
  92.4 1.9 copy-start.6
  282.2 1.0 copy-start.3
  283.7 21.4 %copy-start.2 = (bf16[32,2048]{1,0:T(8,128)(2,1)S(1)}, bf16[32,2048]{1,0:T(8,128)(2,1)}, u32[]{:S(2)}) copy-start(bf16[32,2048]{1,0:T(8,128)(2,1)} %param.24) | copy-start | bytes 393220
  283.7 21.5 %copy-start.5 = (f32[2048]{0:T(1024)S(1)}, f32[2048]{0:T(1024)}, u32[]{:S(2)}) copy-start(f32[2048]{0:T(1024)} %param.27) | copy-start | bytes 24580
  306.5 20.2 %all-to-all-start.2 = ((bf16[8,32,2048]{2,1,0:T(8,128)(2,1)}), bf16[8,32,2048]{2,1,0:T(8,128)(2,1)}, u32[]{:S(2)}, u32[]{:S(2)}) async-start(bf16[8,32,2048]{2,1,0:T(8,128)(2,1)} %broadcast_in_dim.51), calls=%async_computation.2 | async-start | bytes 2097152 | tf_op jit(solution)/shard_map/all_to_all | solution.py:41
  330.5 1.6 copy-start.1
Sparse Core Ops, SparseCore 0:
  9.5 92.9 all-gather.7
  104.6 50.9 all-gather.9
  157.8 51.1 all-gather.5
